TPU v7x, 32 devices: a whole 2x2x4 slice. The times are simulated.
32 devices in a mesh: grp: 2 (over y), sp: 4 (over z), tp: 4 (over x, core).
Axes of the slice: x: 2, y: 2, z: 4, core: 2. Of those that a mesh axis runs over, the one named last changes fastest.
Arguments:
- residual: bfloat16 [2048, 2048], P(('grp', 'sp', 'tp')), parts along dimension 0, may hold values from -6 to 6
- query_nope: bfloat16 [2048, 1024], P(('grp', 'sp'), 'tp'), parts along dimension 0, may hold values from -6 to 6
- query_rope: bfloat16 [2048, 512], P(('grp', 'sp'), 'tp'), parts along dimension 0, may hold values from -240 to 240
- kv_latent: bfloat16 [2048, 256], P(('grp', 'sp')), parts along dimension 0, may hold values from -6 to 6
- rope_key: bfloat16 [2048, 64], P(('grp', 'sp')), parts along dimension 0, may hold values from -6 to 6
- latent_gain: float32 [256], replicated, may hold values from 0.1 to 1.9
- w_key: bfloat16 [256, 1024], P(None, 'tp'), may hold values from -0.375 to 0.375
- w_value: bfloat16 [256, 1024], P(None, 'tp'), may hold values from -0.375 to 0.375
- w_out: bfloat16 [1024, 2048], P('tp'), may hold values from -0.1875 to 0.1875
- post_gain: float32 [2048], replicated, may hold values from 0.1 to 1.9
- routes: int32 [2048, 2], P(('grp', 'sp', 'tp')), parts along dimension 0, may hold values from 0 to 3, all different within a row; in each aligned block of 64 rows (0 to 63, 64 to 127, ...) at most 48 rows name the same one
- route_weight: float32 [2048, 2], P(('grp', 'sp', 'tp')), parts along dimension 0, may hold values from 0.25 to 1
- moe_gain: float32 [2048], replicated, may hold values from 0.1 to 1.9
- w_gate: bfloat16 [4, 2048, 3584], P('sp', None, 'tp'), may hold values from -0.125 to 0.125
- w_up: bfloat16 [4, 2048, 3584], P('sp', None, 'tp'), may hold values from -0.125 to 0.125
- w_down: bfloat16 [4, 3584, 2048], P('sp', 'tp'), may hold values from -0.09375 to 0.09375
Outputs:
- mixed: bfloat16 [2048, 2048], P(('grp', 'sp', 'tp')), parts along dimension 0
There are 2 independent parts, one for each index of `grp`. A program takes and returns all parts, laid end to end along the dimension named above; an argument that names none is the same for every part. Nothing has to cross between parts.
Inputs may be any that keep to these rules, and one draw needn't show every extreme that they name: `routes`: each row names two different experts. Among the 64 rows of one device no expert is named more than 48 times, and some device names some expert exactly 48 times.
All inputs are finite; a program needn't handle non-finite values.
Results may differ from a plain program's by a relative error of at most 0.014.
Values may be sent and summed in bfloat16 or wider, within the bound.
A program may use at most 128 MiB of HBM per device.

v0:
```python
import jax
import jax.numpy as jnp
from jax import lax
from jax.sharding import PartitionSpec as P

HEADS = 8
NOPE = 128
ROPE = 64
VDIM = 128
epsilon = 1e-06
rope_base = 10000.0


def rms_scale(inputs, gain_vector):
    mean_square = jnp.mean(inputs * inputs, axis=-1, keepdims=True)
    return inputs * lax.rsqrt(mean_square + epsilon) * gain_vector


def tables(positions, rot_width):
    frequency = 1.0 / rope_base ** (jnp.arange(0, rot_width, 2, dtype=jnp.float32) / rot_width)
    angles = positions.astype(jnp.float32)[:, None] * frequency[None, :]
    return (jnp.cos(angles), jnp.sin(angles))


def rotate(inputs, cosine_table, sine_table):
    half_width = inputs.shape[-1] // 2
    first_half = inputs[..., :half_width]
    second_half = inputs[..., half_width:]
    return jnp.concatenate(
        [
            first_half * cosine_table - second_half * sine_table,
            second_half * cosine_table + first_half * sine_table,
        ],
        axis=-1,
    )


def expand(latent_rows, rope_rows, latent_gain, w_key, w_value):
    normed = rms_scale(latent_rows.astype(jnp.float32), latent_gain).astype(jnp.bfloat16)
    key_plain = jnp.dot(normed, w_key, preferred_element_type=jnp.float32).astype(jnp.bfloat16)
    value_plain = jnp.dot(normed, w_value, preferred_element_type=jnp.float32).astype(jnp.bfloat16)
    key_positions = jnp.arange(latent_rows.shape[0], dtype=jnp.int32)
    cosine_table, sine_table = tables(key_positions, rope_rows.shape[1])
    key_turned = rotate(rope_rows.astype(jnp.float32), cosine_table, sine_table).astype(
        jnp.bfloat16
    )
    return (key_plain, value_plain, key_turned)


def body(
    residual,
    query_nope,
    query_rope,
    kv_latent,
    rope_key,
    latent_gain,
    w_key,
    w_value,
    w_out,
    post_gain,
    routes,
    route_weight,
    moe_gain,
    w_gate,
    w_up,
    w_down,
):
    tok_rows = query_nope.shape[0]
    heads_here = HEADS // lax.axis_size("tp")
    first_row = lax.axis_index("sp") * tok_rows
    last_row = first_row + tok_rows - 1
    positions = first_row + jnp.arange(tok_rows, dtype=jnp.int32)
    cosine_table, sine_table = tables(positions, ROPE)
    query_plain = query_nope.reshape(tok_rows, heads_here, NOPE)
    query_turned = rotate(
        query_rope.reshape(tok_rows, heads_here, ROPE).astype(jnp.float32),
        cosine_table[:, None, :],
        sine_table[:, None, :],
    ).astype(jnp.bfloat16)
    score_scale = (NOPE + ROPE) ** (-0.5)

    def update(state_now, key_plain, value_plain, key_turned):
        row_max, row_sum, running = state_now
        key_count = key_plain.shape[0]
        key_heads = key_plain.reshape(key_count, heads_here, NOPE)
        value_heads = value_plain.reshape(key_count, heads_here, VDIM)
        scores = jnp.einsum(
            "thd,shd->hts", query_plain, key_heads, preferred_element_type=jnp.float32
        )
        scores = (
            scores
            + jnp.einsum(
                "thd,sd->hts", query_turned, key_turned, preferred_element_type=jnp.float32
            )
        ) * score_scale
        key_positions = jnp.arange(key_count, dtype=jnp.int32)
        allowed = key_positions[None, :] <= positions[:, None]
        scores = jnp.where(allowed[None], scores, -1e30)
        new_max = jnp.maximum(row_max, jnp.max(scores, axis=-1))
        weights = jnp.exp(scores - new_max[..., None])
        row_sum = jnp.sum(weights, axis=-1)
        running = jnp.einsum(
            "hts,shd->htd",
            weights.astype(jnp.bfloat16),
            value_heads,
            preferred_element_type=jnp.float32,
        )
        return (new_max, row_sum, running)

    start_state = (
        jnp.full((heads_here, tok_rows), -1e30, jnp.float32),
        jnp.zeros((heads_here, tok_rows), jnp.float32),
        jnp.zeros((heads_here, tok_rows, VDIM), jnp.float32),
    )
    pieces = (
        lax.all_gather(kv_latent, "sp", axis=0, tiled=True),
        lax.all_gather(rope_key, "sp", axis=0, tiled=True),
    )

    def take_piece(state_in):
        key_plain, value_plain, key_turned = expand(
            pieces[0], pieces[1], latent_gain, w_key, w_value
        )
        return update(state_in, key_plain, value_plain, key_turned)

    def skip_piece(state_in):
        return state_in

    final_state = lax.cond(jnp.int32(0) <= last_row, take_piece, skip_piece, start_state)
    attended = (final_state[2] / final_state[1][..., None]).transpose(1, 0, 2)
    attended = attended.reshape(tok_rows, heads_here * VDIM).astype(jnp.bfloat16)
    chosen = attended
    product = jnp.dot(chosen, w_out, preferred_element_type=jnp.float32)
    branch = lax.psum_scatter(
        product.astype(jnp.bfloat16).astype(jnp.float32).astype(jnp.bfloat16),
        "tp",
        scatter_dimension=0,
        tiled=True,
    ).astype(jnp.float32)
    updated = (residual.astype(jnp.float32) + rms_scale(branch, post_gain)).astype(jnp.bfloat16)
    moe_in = rms_scale(updated.astype(jnp.float32), moe_gain).astype(jnp.bfloat16)
    token_count = routes.shape[0]
    experts = lax.axis_size("sp")
    capacity = max(2, 3 * token_count // experts)
    onehot = (routes[:, :, None] == jnp.arange(experts, dtype=jnp.int32)[None, None, :]).astype(
        jnp.int32
    )
    flat_hits = onehot.reshape(token_count * 2, experts)
    order_in = jnp.cumsum(flat_hits, axis=0) - flat_hits
    slot_ids = jnp.sum(
        (order_in + jnp.arange(experts, dtype=jnp.int32)[None, :] * capacity) * flat_hits, axis=1
    )
    placing = slot_ids[:, None] == jnp.arange(experts * capacity, dtype=jnp.int32)[None, :]
    placing = placing.astype(jnp.bfloat16).reshape(token_count, 2, experts * capacity)
    sending = jnp.einsum("tks,td->sd", placing, moe_in, preferred_element_type=jnp.float32).astype(
        jnp.bfloat16
    )
    received = lax.all_to_all(sending, "sp", split_axis=0, concat_axis=0, tiled=True)
    span_rows = lax.all_gather(received, "tp", axis=0, tiled=True)
    gate_pre = jnp.dot(span_rows, w_gate[0], preferred_element_type=jnp.float32)
    up_proj = jnp.dot(span_rows, w_up[0], preferred_element_type=jnp.float32)
    hidden_rows = (jax.nn.silu(gate_pre) * up_proj).astype(jnp.bfloat16)
    chosen = hidden_rows
    product = jnp.dot(chosen, w_down[0], preferred_element_type=jnp.float32)
    expert_out = lax.psum_scatter(
        product.astype(jnp.bfloat16).astype(jnp.float32).astype(jnp.bfloat16),
        "tp",
        scatter_dimension=0,
        tiled=True,
    )
    returned = lax.all_to_all(expert_out, "sp", split_axis=0, concat_axis=0, tiled=True)
    gathered_back = jnp.einsum("tks,sd->tkd", placing, returned, preferred_element_type=jnp.float32)
    weighted = jnp.sum(gathered_back * route_weight[:, :, None], axis=1)
    return (updated.astype(jnp.float32) + weighted).astype(jnp.bfloat16)


def solution(mesh):
    placed = (
        P(("grp", "sp", "tp"), None),
        P(("grp", "sp"), "tp"),
        P(("grp", "sp"), "tp"),
        P(("grp", "sp"), None),
        P(("grp", "sp"), None),
        P(),
        P(None, "tp"),
        P(None, "tp"),
        P("tp", None),
        P(),
        P(("grp", "sp", "tp"), None),
        P(("grp", "sp", "tp"), None),
        P(),
        P("sp", None, "tp"),
        P("sp", None, "tp"),
        P("sp", "tp", None),
    )
    return jax.shard_map(
        body, mesh=mesh, in_specs=placed, out_specs=P(("grp", "sp", "tp"), None), check_vma=False
    )
```

profile of v0, /device:TPU:0, one launch (start us, length us, event | category | flops | bytes accessed | tf_op | source)
XLA Modules:
  0.0 215.7 jit_solution(12267878147756269615)
XLA Ops:
  6.6 1.0 copy.40
  7.6 15.3 %all_gather.10 = bf16[1024,64]{0,1:T(8,128)(2,1)S(1)} all-gather(bf16[256,64]{0,1:T(8,128)(2,1)} %param.22), channel_id=1, replica_groups=mesh['grp'=2,'sp'=4,'tp'=4] {'sp'}, dimensions={0}, use_global_device_ids=true | all-gather | bytes 163840 | tf_op jit(solution)/shard_map/all_gather | solution.py:117
  22.9 16.2 %all_gather.9 = bf16[1024,256]{1,0:T(8,128)(2,1)S(1)} all-gather(bf16[256,256]{1,0:T(8,128)(2,1)} %param.21), channel_id=1, replica_groups=mesh['grp'=2,'sp'=4,'tp'=4] {'sp'}, dimensions={0}, use_global_device_ids=true | all-gather | bytes 655360 | tf_op jit(solution)/shard_map/all_gather | solution.py:116
  39.1 0.2 multiply_cosine_fusion.1
  39.3 4.9 %conditional.1 = (f32[2,256]{1,0:T(2,128)S(1)}, f32[2,256,128]{1,2,0:T(8,128)S(1)}) conditional(s32[]{:T(128)} %convert_element_type.105, () %tuple.13, (s32[]{:T(128)}, s32[256]{0:T(256)S(1)}, bf16[1024,256]{1,0:T(8,128)(2,1)S(1)}, f32[256]{0:T(256)}, bf16[256,256]{1,0:T(8,128)(2,1)}, /*index=5*/bf16[256,256]{1,0:T(8,128)(2,1)}, ...), branch_computations={%region_0.0_spmd, %region_1.5_spmd} | conditional | flops 612468544 | bytes 17417576 | solution.py:129
  39.4 0.2 fusion.4
  39.6 0.2 iota_compare_fusion
  39.9 0.6 fusion.17
  40.4 1.4 convolution_convert_fusion
  41.9 0.5 convolution_convert_fusion.1
  42.4 0.5 fusion.20
  42.9 0.6 fusion.58
  43.4 0.5 fusion.7
  43.9 0.3 fusion.3
  44.3 1.5 convolution_convert_fusion.2
  46.0 0.1 eq.54
  46.2 0.2 reduce_window_sum.11
  46.4 0.2 select_reduce_fusion
  46.5 0.1 eq.58
  46.8 0.1 convert_reduce_fusion
  46.9 24.3 %reduce-scatter.3.cloned.1.call-done = bf16[64,2048]{1,0:T(8,128)(2,1)} async-done(((bf16[256,2048]{1,0:T(8,128)(2,1)}), bf16[64,2048]{1,0:T(8,128)(2,1)}) %reduce-scatter.3.cloned.1.call-update) | async-done | bytes 262160 | tf_op jit(solution)/shard_map/reduce_scatter | solution.py:134
  71.2 1.1 fusion.40
  72.3 1.2 fusion.44
  73.6 0.4 convolution_convert_fusion.3
  74.0 24.4 %all_to_all.24 = bf16[4,48,2048]{2,1,0:T(8,128)(2,1)} all-to-all(bf16[4,48,2048]{2,1,0:T(8,128)(2,1)S(1)} %bitcast.63), channel_id=1, replica_groups=mesh['grp'=2,'sp'=4,'tp'=4] {'sp'}, dimensions={0} | all-to-all | bytes 1572864 | tf_op jit(solution)/shard_map/all_to_all | solution.py:158
  98.5 26.7 %all-gather.2.cloned.1.call-done = bf16[768,2048]{1,0:T(8,128)(2,1)} async-done(((bf16[192,2048]{1,0:T(8,128)(2,1)}), bf16[768,2048]{1,0:T(8,128)(2,1)}) %all-gather.2.cloned.1.call-update) | async-done | bytes 3145744 | tf_op jit(solution)/shard_map/all_gather | solution.py:159
  125.3 8.0 %fusion.28 = f32[768,896]{1,0:T(8,128)} fusion(bf16[768,2048]{1,0:T(8,128)(2,1)} %all-gather.2.cloned.1.call-done, bf16[1,2048,896]{2,1,0:T(8,128)(2,1)} %param.32), kind=kOutput, calls=%fused_computation.40 | convolution fusion | flops 2818572288 | bytes 9568256 | tf_op jit(solution)/shard_map/dot_general | solution.py:161
  133.3 12.2 %fusion.32 = bf16[768,2048]{1,0:T(8,128)(2,1)} fusion(bf16[1,896,2048]{2,1,0:T(8,128)(2,1)} %param.33, f32[768,896]{1,0:T(8,128)} %fusion.28, bf16[768,2048]{1,0:T(8,128)(2,1)} %all-gather.2.cloned.1.call-done, bf16[1,2048,896]{2,1,0:T(8,128)(2,1)} %param.31), kind=kOutput, calls=%fused_computation.44 | convolution fusion | flops 5642846208 | bytes 16384000 | tf_op jit(solution)/shard_map/dot_general | solution.py:164
  145.5 38.1 %reduce-scatter.5.cloned.1.call-done = bf16[192,2048]{1,0:T(8,128)(2,1)} async-done(((bf16[768,2048]{1,0:T(8,128)(2,1)}), bf16[192,2048]{1,0:T(8,128)(2,1)}) %reduce-scatter.5.cloned.1.call-update) | async-done | bytes 786448 | tf_op jit(solution)/shard_map/reduce_scatter | solution.py:165
  183.5 24.5 %all_to_all.25 = bf16[4,48,2048]{2,1,0:T(8,128)(2,1)S(1)} all-to-all(bf16[4,48,2048]{2,1,0:T(8,128)(2,1)} %bitcast.64), channel_id=1, replica_groups=mesh['grp'=2,'sp'=4,'tp'=4] {'sp'}, dimensions={0} | all-to-all | bytes 1572864 | tf_op jit(solution)/shard_map/all_to_all | solution.py:171
  208.1 0.4 fusion.37
  208.4 0.8 fusion.47
  (42 shorter events, 0.6 us)
Async XLA Ops:
  6.5 37.8 %copy-start = (bf16[256,2048]{1,0:T(8,128)(2,1)S(1)}, bf16[256,2048]{1,0:T(8,128)(2,1)}, u32[]{:S(2)}) copy-start(bf16[256,2048]{1,0:T(8,128)(2,1)} %param.26) | copy-start | bytes 3145732
  6.5 64.6 %reduce-scatter.3.cloned.1.call-start = ((), (), s32[]{:S(2)}) async-start(), calls=%async_computation.4 | async-start | bytes 1310720 | tf_op jit(solution)/shard_map/reduce_scatter | solution.py:134
  39.3 2.5 %copy-start.7 = (bf16[256,256]{1,0:T(8,128)(2,1)S(1)}, bf16[256,256]{1,0:T(8,128)(2,1)}, u32[]{:S(2)}) copy-start(bf16[256,256]{1,0:T(8,128)(2,1)} %get-tuple-element.44) | copy-start | bytes 393220 | tf_op jit(solution)/shard_map/cond
  39.4 2.5 %copy-start.8 = (f32[256]{0:T(256)S(1)}, f32[256]{0:T(256)}, u32[]{:S(2)}) copy-start(f32[256]{0:T(256)} %get-tuple-element.43) | copy-start | bytes 3076 | tf_op jit(solution)/shard_map/cond
  39.4 3.0 %copy-start.2 = (bf16[256,256]{1,0:T(8,128)(2,1)S(1)}, bf16[256,256]{1,0:T(8,128)(2,1)}, u32[]{:S(2)}) copy-start(bf16[256,256]{1,0:T(8,128)(2,1)} %get-tuple-element.45) | copy-start | bytes 393220 | tf_op jit(solution)/shard_map/cond
  44.2 1.6 copy-start.6
  44.2 28.0 %copy-start.1 = (bf16[64,2048]{1,0:T(8,128)(2,1)S(1)}, bf16[64,2048]{1,0:T(8,128)(2,1)}, u32[]{:S(2)}) copy-start(bf16[64,2048]{1,0:T(8,128)(2,1)} %param.18) | copy-start | bytes 786436
  44.2 28.0 %copy-start.3 = (f32[2048]{0:T(1024)S(1)}, f32[2048]{0:T(1024)}, u32[]{:S(2)}) copy-start(f32[2048]{0:T(1024)} %param.27) | copy-start | bytes 24580
  44.3 29.3 %copy-start.4 = (f32[2048]{0:T(1024)S(1)}, f32[2048]{0:T(1024)}, u32[]{:S(2)}) copy-start(f32[2048]{0:T(1024)} %param.30) | copy-start | bytes 24580
  45.8 79.5 %all-gather.2.cloned.1.call-start = ((), (), s32[]{:S(2)}) async-start(), calls=%async_computation.5 | async-start | bytes 3932160 | tf_op jit(solution)/shard_map/all_gather | solution.py:159
  98.5 85.1 %reduce-scatter.5.cloned.1.call-start = ((), (), s32[]{:S(2)}) async-start(), calls=%async_computation.6 | async-start | bytes 3932160 | tf_op jit(solution)/shard_map/reduce_scatter | solution.py:165
  145.4 62.6 %copy-start.5 = (f32[64,2]{0,1:T(2,128)S(1)}, f32[64,2]{0,1:T(2,128)}, u32[]{:S(2)}) copy-start(f32[64,2]{0,1:T(2,128)} %param.29) | copy-start | bytes 1540
Sparse Core Ops, SparseCore 0:
  45.9 25.1 reduce-scatter.2
  98.6 26.6 all-gather.1
  145.6 37.9 reduce-scatter.4
where the time goes:
time: 216 us
  waiting for transfers between devices  89.2 us (41%)
  blocking collectives  80.5 us (37%)
  matrix products  25.8 us (12%)
  between operations  13.3 us (6%)
  other arithmetic  5.23 us (2%)
    reduce_scatter x2, waiting for transfers between devices, body(): lax.psum_scatter(product.astype(jnp.bfloat16).astype(jnp.float32).astype(...  62.4 us
    all_gather x1, waiting for transfers between devices, body(): span_rows = lax.all_gather(received, 'tp', axis=0, tiled=True)  26.7 us
    all_to_all x1, blocking collectives, body(): lax.all_to_all(expert_out, 'sp', split_axis=0, concat_axis=0, tiled=True)  24.5 us
    all_to_all x1, blocking collectives, body(): lax.all_to_all(sending, 'sp', split_axis=0, concat_axis=0, tiled=True)  24.4 us
    all_gather x1, blocking collectives, body(): lax.all_gather(kv_latent, 'sp', axis=0, tiled=True)  16.2 us
    all_gather x1, blocking collectives, body(): lax.all_gather(rope_key, 'sp', axis=0, tiled=True)  15.3 us
    dot_general x1, matrix products, body(): product = jnp.dot(chosen, w_down[0], preferred_element_type=jnp.float32)  12.2 us
    dot_general x1, matrix products, body(): up_proj = jnp.dot(span_rows, w_up[0], preferred_element_type=jnp.float32)  8 us
  transfers between devices with their start and end apart: 3, of which 3 were waited for; matrix products, arithmetic and copies ran while one was open for 0% of the time, Pallas kernels for 0%

commit v1 on v0

--- a/solution.py
+++ b/solution.py
@@ -9,6 +9,16 @@
 VDIM = 128
 epsilon = 1e-06
 rope_base = 10000.0
+
+
+def around_the_ring(x, name, dim):
+    count = lax.axis_size(name)
+    current, tiles = (x, [x])
+    for _ in range(count - 1):
+        current = lax.ppermute(current, name, [(i, (i + 1) % count) for i in range(count)])
+        tiles.insert(0, current)
+    line = jnp.concatenate(tiles, axis=dim)
+    return jnp.roll(line, (lax.axis_index(name) + 1) * x.shape[dim], axis=dim)
 
 
 def rms_scale(inputs, gain_vector):
@@ -156,7 +166,7 @@
         jnp.bfloat16
     )
     received = lax.all_to_all(sending, "sp", split_axis=0, concat_axis=0, tiled=True)
-    span_rows = lax.all_gather(received, "tp", axis=0, tiled=True)
+    span_rows = around_the_ring(received, "tp", 0)
     gate_pre = jnp.dot(span_rows, w_gate[0], preferred_element_type=jnp.float32)
     up_proj = jnp.dot(span_rows, w_up[0], preferred_element_type=jnp.float32)
     hidden_rows = (jax.nn.silu(gate_pre) * up_proj).astype(jnp.bfloat16)

time: 216 us -> 225 us (1.042)
  local copies, waits for them, and re-layouts: 1.52 us -> 7.12 us
  waiting for transfers between devices: 89.2 us -> 94.8 us
    ppermute x0 -> x3, waiting for transfers between devices: none -> 34.3 us  [around_the_ring(): lax.ppermute(current, name, [(i, (i + 1) % count) for i in range(count)])]
    all_gather x1 -> x0, waiting for transfers between devices: 26.7 us -> none  [body(): span_rows = lax.all_gather(received, 'tp', axis=0, tiled=True)]
    unnamed x13 -> x28, local copies, waits for them, and re-layouts: 0.13 us -> 5.67 us
    dot_general x1, matrix products: 8 us -> 4.91 us  [body(): up_proj = jnp.dot(span_rows, w_up[0], preferred_element_type=jnp.float32)]
  transfers between devices with their start and end apart: 3 -> 5, of which waited for: 3 -> 5; matrix products, arithmetic and copies ran while one was open for 0% -> 0% of each run, Pallas kernels for 0% -> 0%
where the time goes in v1:
time: 225 us
  waiting for transfers between devices  94.8 us (42%)
  blocking collectives  80.4 us (36%)
  matrix products  23.8 us (11%)
  between operations  13.7 us (6%)
  local copies, waits for them, and re-layouts  7.12 us (3%)
  other arithmetic  5.22 us (2%)
    reduce_scatter x2, waiting for transfers between devices, body(): lax.psum_scatter(product.astype(jnp.bfloat16).astype(jnp.float32).astype(...  60.4 us
    ppermute x3, waiting for transfers between devices, around_the_ring(): lax.ppermute(current, name, [(i, (i + 1) % count) for i in range(count)])  34.3 us
    all_to_all x1, blocking collectives, body(): lax.all_to_all(expert_out, 'sp', split_axis=0, concat_axis=0, tiled=True)  24.5 us
    all_to_all x1, blocking collectives, body(): lax.all_to_all(sending, 'sp', split_axis=0, concat_axis=0, tiled=True)  24.3 us
    all_gather x1, blocking collectives, body(): lax.all_gather(kv_latent, 'sp', axis=0, tiled=True)  16.2 us
    all_gather x1, blocking collectives, body(): lax.all_gather(rope_key, 'sp', axis=0, tiled=True)  15.3 us
    dot_general x1, matrix products, body(): product = jnp.dot(chosen, w_down[0], preferred_element_type=jnp.float32)  12.2 us
    unnamed x28, local copies, waits for them, and re-layouts  5.67 us
  transfers between devices with their start and end apart: 5, of which 5 were waited for; matrix products, arithmetic and copies ran while one was open for 0% of the time, Pallas kernels for 0%

profile of v1, /device:TPU:0, one launch (start us, length us, event | category | flops | bytes accessed | tf_op | source)
XLA Modules:
  0.0 225.1 jit_solution(2556440639576791712)
XLA Ops:
  6.6 1.0 copy.40
  7.6 15.3 %all_gather.7 = bf16[1024,64]{0,1:T(8,128)(2,1)S(1)} all-gather(bf16[256,64]{0,1:T(8,128)(2,1)} %param.22), channel_id=1, replica_groups=mesh['grp'=2,'sp'=4,'tp'=4] {'sp'}, dimensions={0}, use_global_device_ids=true | all-gather | bytes 163840 | tf_op jit(solution)/shard_map/all_gather | solution.py:127
  22.9 16.2 %all_gather.6 = bf16[1024,256]{1,0:T(8,128)(2,1)S(1)} all-gather(bf16[256,256]{1,0:T(8,128)(2,1)} %param.21), channel_id=1, replica_groups=mesh['grp'=2,'sp'=4,'tp'=4] {'sp'}, dimensions={0}, use_global_device_ids=true | all-gather | bytes 655360 | tf_op jit(solution)/shard_map/all_gather | solution.py:126
  39.1 0.2 multiply_cosine_fusion.1
  39.3 5.8 %conditional.1 = (f32[2,256]{1,0:T(2,128)S(1)}, f32[2,256,128]{1,2,0:T(8,128)S(1)}) conditional(s32[]{:T(128)} %convert_element_type.105, () %tuple.13, (s32[]{:T(128)}, s32[256]{0:T(256)S(1)}, bf16[1024,256]{1,0:T(8,128)(2,1)S(1)}, f32[256]{0:T(256)}, bf16[256,256]{1,0:T(8,128)(2,1)}, /*index=5*/bf16[256,256]{1,0:T(8,128)(2,1)}, ...), branch_computations={%region_0.0_spmd, %region_1.5_spmd} | conditional | flops 612468544 | bytes 16889136 | solution.py:139
  39.4 0.2 fusion.4
  39.8 0.6 fusion.17
  40.4 1.4 convolution_convert_fusion
  41.8 1.4 convolution_convert_fusion.1
  43.2 0.5 fusion.20
  43.7 0.6 fusion.68
  44.3 0.5 fusion.7
  44.8 0.3 fusion.3
  45.2 1.5 convolution_convert_fusion.2
  47.2 0.2 select_reduce_fusion
  47.8 24.3 %reduce-scatter.3.cloned.1.call-done = bf16[64,2048]{1,0:T(8,128)(2,1)} async-done(((bf16[256,2048]{1,0:T(8,128)(2,1)}), bf16[64,2048]{1,0:T(8,128)(2,1)}) %reduce-scatter.3.cloned.1.call-update) | async-done | bytes 262160 | tf_op jit(solution)/shard_map/reduce_scatter | solution.py:144
  72.0 1.1 fusion.47
  73.2 1.2 fusion.51
  74.4 0.4 convolution_convert_fusion.3
  74.9 24.3 %all_to_all.24 = bf16[4,48,2048]{2,1,0:T(8,128)(2,1)S(1)} all-to-all(bf16[4,48,2048]{2,1,0:T(8,128)(2,1)S(1)} %bitcast.63), channel_id=1, replica_groups=mesh['grp'=2,'sp'=4,'tp'=4] {'sp'}, dimensions={0} | all-to-all | bytes 1572864 | tf_op jit(solution)/shard_map/all_to_all | solution.py:168
  99.2 11.4 %collective-permute-done = bf16[192,2048]{1,0:T(8,128)(2,1)S(1)} collective-permute-done((bf16[192,2048]{1,0:T(8,128)(2,1)S(1)}, bf16[192,2048]{1,0:T(8,128)(2,1)S(1)}, u32[]{:S(2)}, u32[]{:S(2)}) %collective-permute-start) | collective-permute-done | bytes 786464 | tf_op jit(solution)/shard_map/ppermute | solution.py:18
  110.6 11.4 %collective-permute-done.1 = bf16[192,2048]{1,0:T(8,128)(2,1)S(1)} collective-permute-done((bf16[192,2048]{1,0:T(8,128)(2,1)S(1)}, bf16[192,2048]{1,0:T(8,128)(2,1)S(1)}, u32[]{:S(2)}, u32[]{:S(2)}) %collective-permute-start.1) | collective-permute-done | bytes 786464 | tf_op jit(solution)/shard_map/ppermute | solution.py:18
  122.0 11.5 %collective-permute-done.2 = bf16[192,2048]{1,0:T(8,128)(2,1)} collective-permute-done((bf16[192,2048]{1,0:T(8,128)(2,1)S(1)}, bf16[192,2048]{1,0:T(8,128)(2,1)}, u32[]{:S(2)}, u32[]{:S(2)}) %collective-permute-start.2) | collective-permute-done | bytes 786464 | tf_op jit(solution)/shard_map/ppermute | solution.py:18
  133.6 1.2 constant_dynamic-update-slice_fusion.7
  135.0 1.3 constant_dynamic-update-slice_fusion.3
  136.6 2.7 %copy-done.5 = bf16[1536,2048]{1,0:T(8,128)(2,1)} copy-done((bf16[1536,2048]{1,0:T(8,128)(2,1)}, bf16[1536,2048]{1,0:T(8,128)(2,1)S(1)}, u32[]{:S(2)}) %copy-start.5) | copy-done | bytes 6291480
  139.2 4.9 %fusion.28 = f32[768,896]{1,0:T(8,128)} fusion(bf16[1,2048,896]{2,1,0:T(8,128)(2,1)S(1)} %copy-done.10, bf16[1536,2048]{1,0:T(8,128)(2,1)S(1)} %constant_dynamic-update-slice_fusion, s32[]{:T(128)S(6)} %select_n.18), kind=kOutput, calls=%fused_computation.40 | convolution fusion | flops 2818572288 | bytes 9568260 | tf_op jit(solution)/shard_map/dot_general | solution.py:171
  144.1 12.2 %fusion.32 = bf16[768,2048]{1,0:T(8,128)(2,1)} fusion(bf16[1,896,2048]{2,1,0:T(8,128)(2,1)} %param.33, f32[768,896]{1,0:T(8,128)} %fusion.28, bf16[1,2048,896]{2,1,0:T(8,128)(2,1)} %param.31, bf16[1536,2048]{1,0:T(8,128)(2,1)} %copy-done.5, s32[]{:T(128)S(6)} %select_n.18), kind=kOutput, calls=%fused_computation.44 | convolution fusion | flops 5642846208 | bytes 16384004 | tf_op jit(solution)/shard_map/dot_general | solution.py:174
  156.4 36.2 %reduce-scatter.5.cloned.1.call-done = bf16[192,2048]{1,0:T(8,128)(2,1)} async-done(((bf16[768,2048]{1,0:T(8,128)(2,1)}), bf16[192,2048]{1,0:T(8,128)(2,1)}) %reduce-scatter.5.cloned.1.call-update) | async-done | bytes 786448 | tf_op jit(solution)/shard_map/reduce_scatter | solution.py:175
  192.6 24.5 %all_to_all.25 = bf16[4,48,2048]{2,1,0:T(8,128)(2,1)S(1)} all-to-all(bf16[4,48,2048]{2,1,0:T(8,128)(2,1)} %bitcast.64), channel_id=1, replica_groups=mesh['grp'=2,'sp'=4,'tp'=4] {'sp'}, dimensions={0} | all-to-all | bytes 1572864 | tf_op jit(solution)/shard_map/all_to_all | solution.py:181
  217.1 0.4 fusion.38
  217.5 0.8 fusion.54
  (57 shorter events, 1.7 us)
Async XLA Ops:
  6.5 38.7 %copy-start = (bf16[256,2048]{1,0:T(8,128)(2,1)S(1)}, bf16[256,2048]{1,0:T(8,128)(2,1)}, u32[]{:S(2)}) copy-start(bf16[256,2048]{1,0:T(8,128)(2,1)} %param.26) | copy-start | bytes 3145732
  6.5 65.5 %reduce-scatter.3.cloned.1.call-start = ((), (), s32[]{:S(2)}) async-start(), calls=%async_computation.4 | async-start | bytes 1310720 | tf_op jit(solution)/shard_map/reduce_scatter | solution.py:144
  39.3 3.9 %copy-start.4 = (bf16[256,256]{1,0:T(8,128)(2,1)S(1)}, bf16[256,256]{1,0:T(8,128)(2,1)}, u32[]{:S(2)}) copy-start(bf16[256,256]{1,0:T(8,128)(2,1)} %get-tuple-element.45) | copy-start | bytes 393220 | tf_op jit(solution)/shard_map/cond
  45.1 1.6 copy-start.9
  45.1 28.0 %copy-start.3 = (bf16[64,2048]{1,0:T(8,128)(2,1)S(1)}, bf16[64,2048]{1,0:T(8,128)(2,1)}, u32[]{:S(2)}) copy-start(bf16[64,2048]{1,0:T(8,128)(2,1)} %param.18) | copy-start | bytes 786436
  45.1 28.0 %copy-start.6 = (f32[2048]{0:T(1024)S(1)}, f32[2048]{0:T(1024)}, u32[]{:S(2)}) copy-start(f32[2048]{0:T(1024)} %param.27) | copy-start | bytes 24580
  45.1 29.3 %copy-start.7 = (f32[2048]{0:T(1024)S(1)}, f32[2048]{0:T(1024)}, u32[]{:S(2)}) copy-start(f32[2048]{0:T(1024)} %param.30) | copy-start | bytes 24580
  46.7 145.9 %reduce-scatter.5.cloned.1.call-start = ((), (), s32[]{:S(2)}) async-start(), calls=%async_computation.5 | async-start | bytes 3932160 | tf_op jit(solution)/shard_map/reduce_scatter | solution.py:175
  74.4 47.6 %copy-start.1 = (bf16[64,2048]{1,0:T(8,128)(2,1)}, bf16[64,2048]{1,0:T(8,128)(2,1)S(1)}, u32[]{:S(2)}) copy-start(bf16[64,2048]{1,0:T(8,128)(2,1)S(1)} %get-tuple-element.49) | copy-start | bytes 786436
  99.2 11.4 %collective-permute-start = (bf16[192,2048]{1,0:T(8,128)(2,1)S(1)}, bf16[192,2048]{1,0:T(8,128)(2,1)S(1)}, u32[]{:S(2)}, u32[]{:S(2)}) collective-permute-start(bf16[192,2048]{1,0:T(8,128)(2,1)S(1)} %bitcast.59), channel_id=1, source_target_pairs={{0,1},{1,2},{2,3},{3,0},{4,5},{5,6},{6,7},{7,4},{8,9},{9,10},{10,1... | collective-permute-start | bytes 2359304 | tf_op jit(solution)/shard_map/ppermute | solution.py:18
  110.6 11.4 %collective-permute-start.1 = (bf16[192,2048]{1,0:T(8,128)(2,1)S(1)}, bf16[192,2048]{1,0:T(8,128)(2,1)S(1)}, u32[]{:S(2)}, u32[]{:S(2)}) collective-permute-start(bf16[192,2048]{1,0:T(8,128)(2,1)S(1)} %collective-permute-done), channel_id=1, source_target_pairs={{0,1},{1,2},{2,3},{3,0},{4,5},{5,6},{6,7},{7,4},{8,9},{9,10},{10,1... | collective-permute-start | bytes 2359304 | tf_op jit(solution)/shard_map/ppermute | solution.py:18
  122.0 11.5 %collective-permute-start.2 = (bf16[192,2048]{1,0:T(8,128)(2,1)S(1)}, bf16[192,2048]{1,0:T(8,128)(2,1)}, u32[]{:S(2)}, u32[]{:S(2)}) collective-permute-start(bf16[192,2048]{1,0:T(8,128)(2,1)S(1)} %collective-permute-done.1), channel_id=1, source_target_pairs={{0,1},{1,2},{2,3},{3,0},{4,5},{5,6},{6,7},{7,4},{8,9},{9,10},{10,1... | collective-permute-start | bytes 2359304 | tf_op jit(solution)/shard_map/ppermute | solution.py:18
  134.9 4.3 %copy-start.10 = (bf16[1,2048,896]{2,1,0:T(8,128)(2,1)S(1)}, bf16[1,2048,896]{2,1,0:T(8,128)(2,1)}, u32[]{:S(2)}) copy-start(bf16[1,2048,896]{2,1,0:T(8,128)(2,1)} %param.32) | copy-start | bytes 11010052
  136.6 2.7 %copy-start.5 = (bf16[1536,2048]{1,0:T(8,128)(2,1)}, bf16[1536,2048]{1,0:T(8,128)(2,1)S(1)}, u32[]{:S(2)}) copy-start(bf16[1536,2048]{1,0:T(8,128)(2,1)S(1)} %constant_dynamic-update-slice_fusion) | copy-start | bytes 18874372
  156.4 60.7 %copy-start.8 = (f32[64,2]{0,1:T(2,128)S(1)}, f32[64,2]{0,1:T(2,128)}, u32[]{:S(2)}) copy-start(f32[64,2]{0,1:T(2,128)} %param.29) | copy-start | bytes 1540
  156.4 61.1 %copy-start.2 = (bf16[64,2048]{1,0:T(8,128)(2,1)S(1)}, bf16[64,2048]{1,0:T(8,128)(2,1)}, u32[]{:S(2)}) copy-start(bf16[64,2048]{1,0:T(8,128)(2,1)} %copy-done.1) | copy-start | bytes 786436
Sparse Core Ops, SparseCore 0:
  46.8 25.1 reduce-scatter.2
  156.5 35.9 reduce-scatter.4
